TPU v7x, 32 devices: a whole 2x2x4 slice. The times are simulated.
32 devices in a mesh: grp: 2 (over x), ep: 16 (over z, y, core).
Axes of the slice: x: 2, y: 2, z: 4, core: 2. Of those that a mesh axis runs over, the one named last changes fastest.
Arguments:
- stream: bfloat16 [32, 2048], P('grp', 'ep'), parts along dimension 0, may hold values from -48 to 48
- conv_cache: bfloat16 [32, 3, 2560], P(('grp', 'ep')), parts along dimension 0, may hold values from -6 to 6
- scan_state: float32 [32, 32, 64, 128], P(('grp', 'ep')), parts along dimension 0, may hold values from -4 to 4
- gate_weight: bfloat16 [2048, 2048], P('ep'), may hold values from -0.125 to 0.125
- value_weight: bfloat16 [2048, 2048], P('ep'), may hold values from -0.125 to 0.125
- entry_weight: bfloat16 [2048, 256], P('ep'), may hold values from -0.125 to 0.125
- readout_weight: bfloat16 [2048, 256], P('ep'), may hold values from -0.125 to 0.125
- step_weight: bfloat16 [2048, 32], P('ep'), may hold values from -0.125 to 0.125
- conv_weight: bfloat16 [4, 2560], replicated, may hold values from -3 to 3
- step_bias: float32 [32], replicated, may hold values from -4 to -1
- decay_rate: float32 [32], replicated, may hold values from 0.5 to 8
- skip_gain: float32 [32], replicated, may hold values from 0.1 to 1.9
- group_gain: float32 [2048], replicated, may hold values from 0.1 to 1.9
- out_weight: bfloat16 [2048, 2048], P(None, 'ep'), may hold values from -0.125 to 0.125
- first_gain: float32 [2048], replicated, may hold values from 0.1 to 1.9
- routes: int32 [32, 4], P('grp'), parts along dimension 0, may hold values from 0 to 15, all different within a row; in each aligned block of 16 rows (0 to 15, 16 to 31, ...) at most 8 rows name the same one
- route_weight: float32 [32, 4], P('grp'), parts along dimension 0, may hold values from 0.1 to 1
- expert_gate: bfloat16 [16, 2048, 256], P('ep'), may hold values from -0.125 to 0.125
- expert_up: bfloat16 [16, 2048, 256], P('ep'), may hold values from -0.125 to 0.125
- expert_down: bfloat16 [16, 256, 2048], P('ep'), may hold values from -0.375 to 0.375
- shared_gate: bfloat16 [2048, 256], replicated, may hold values from -0.125 to 0.125
- shared_up: bfloat16 [2048, 256], replicated, may hold values from -0.125 to 0.125
- shared_down: bfloat16 [256, 2048], replicated, may hold values from -0.375 to 0.375
- second_gain: float32 [2048], P('ep'), may hold values from 0.1 to 1.9
Outputs:
- result: bfloat16 [32, 2048], P('grp', 'ep'), parts along dimension 0
- new_conv: bfloat16 [32, 3, 2560], P(('grp', 'ep')), parts along dimension 0
- new_state: float32 [32, 32, 64, 128], P(('grp', 'ep')), parts along dimension 0
There are 2 independent parts, one for each index of `grp`. A program takes and returns all parts, laid end to end along the dimension named above; an argument that names none is the same for every part. Nothing has to cross between parts.
Inputs may be any that keep to these rules, and one draw needn't show every extreme that they name: `routes`: each row names 4 different experts; no expert is named by more than 8 rows, a bound that some block reaches.
All inputs are finite; a program needn't handle non-finite values.
Results may differ from a plain program's by a relative error of at most 0.0065.
Values may be sent and summed in bfloat16 or wider, within the bound.
A program may use at most 64 MiB of HBM per device.

v0:
```python
import jax
import jax.numpy as jnp
from jax import lax
from jax.sharding import PartitionSpec as P

HEAD_DIM = 64
STATE = 128
GROUPS = 2
CAP = 8
RESIDUAL_SCALE = 2.0**0.25
NORM_EPSILON = 1e-05
GATED_EPSILON = 1e-06


def rounded(value):
    return lax.optimization_barrier(value.astype(jnp.bfloat16))


def finish_norm(residual, row_total, square, full_width, gain):
    mean_value = (row_total / full_width)[:, None]
    variance = (square / full_width)[:, None] - mean_value * mean_value
    return (residual - mean_value) * lax.rsqrt(variance + NORM_EPSILON) * gain


def swiglu(inputs, gate_matrix, up_matrix, down_matrix):
    hidden = (
        jax.nn.silu(jnp.dot(inputs, gate_matrix, preferred_element_type=jnp.float32))
        * jnp.dot(inputs, up_matrix, preferred_element_type=jnp.float32)
    ).astype(jnp.bfloat16)
    return rounded(jnp.dot(hidden, down_matrix, preferred_element_type=jnp.float32))


def on_device(
    stream,
    conv_cache,
    scan_state,
    gate_weight,
    value_weight,
    entry_weight,
    readout_weight,
    step_weight,
    conv_weight,
    step_bias,
    decay_rate,
    skip_gain,
    group_gain,
    out_weight,
    first_gain,
    routes,
    route_weight,
    expert_gate,
    expert_up,
    expert_down,
    shared_gate,
    shared_up,
    shared_down,
    second_gain,
):
    devices = lax.axis_size("ep")
    device_rank = lax.axis_index("ep")
    own_rows = conv_cache.shape[0]
    row_count = stream.shape[0]
    slice_width = stream.shape[1]
    full_width = slice_width * devices
    inner_width = gate_weight.shape[1]
    head_count = step_weight.shape[1]
    per_group = head_count // GROUPS
    group_width = inner_width // GROUPS
    bounds = (inner_width, 2 * inner_width + 2 * GROUPS * STATE)
    weights_in = (gate_weight, value_weight, entry_weight, readout_weight, step_weight)
    summed = rounded(
        lax.psum_scatter(
            jnp.concatenate(
                [
                    jnp.dot(stream, weight, preferred_element_type=jnp.float32)
                    for weight in weights_in
                ],
                axis=1,
            ),
            "ep",
            scatter_dimension=0,
            tiled=True,
        )
    )
    gate_rows = summed[:, : bounds[0]]
    fresh = summed[:, bounds[0] : bounds[1]]
    step_rows = summed[:, bounds[1] :]
    window = jnp.concatenate([conv_cache, fresh[:, None, :]], axis=1)
    active = jax.nn.silu(
        jnp.sum(window.astype(jnp.float32) * conv_weight.astype(jnp.float32)[None], axis=1)
    )
    head_in = active[:, :inner_width].reshape(own_rows, GROUPS, per_group, HEAD_DIM)
    entry_rows = active[:, inner_width : inner_width + GROUPS * STATE].reshape(
        own_rows, GROUPS, 1, 1, STATE
    )
    readout_rows = active[:, inner_width + GROUPS * STATE :].reshape(own_rows, GROUPS, 1, 1, STATE)
    step_size = jax.nn.softplus(step_rows.astype(jnp.float32) + step_bias).reshape(
        own_rows, GROUPS, per_group
    )
    retained = jnp.exp(-step_size * decay_rate.reshape(GROUPS, per_group))
    old_state = scan_state.reshape(own_rows, GROUPS, per_group, HEAD_DIM, STATE)
    new_state = (
        retained[..., None, None] * old_state
        + (step_size[..., None] * head_in)[..., None] * entry_rows
    )
    head_out = (
        jnp.sum(new_state * readout_rows, axis=-1)
        + skip_gain.reshape(GROUPS, per_group)[:, :, None] * head_in
    )
    gated_out = head_out.reshape(own_rows, GROUPS, group_width) * jax.nn.silu(
        gate_rows.astype(jnp.float32)
    ).reshape(own_rows, GROUPS, group_width)
    normed = gated_out * lax.rsqrt(
        jnp.mean(gated_out * gated_out, axis=-1, keepdims=True) + GATED_EPSILON
    )
    normed = (normed.reshape(own_rows, inner_width) * group_gain).astype(jnp.bfloat16)
    mixer_out = rounded(
        jnp.dot(
            lax.all_gather(normed, "ep", axis=0, tiled=True),
            out_weight,
            preferred_element_type=jnp.float32,
        )
    )
    column_start = device_rank * slice_width
    residual = RESIDUAL_SCALE * stream.astype(jnp.float32) + mixer_out.astype(jnp.float32)
    row_total, square = lax.psum(
        (jnp.sum(residual, axis=1), jnp.sum(residual * residual, axis=1)), "ep"
    )
    gain_part = lax.dynamic_slice_in_dim(first_gain, column_start, slice_width, 0)
    first_part = rounded(finish_norm(residual, row_total, square, full_width, gain_part))
    first_rows = lax.all_gather(first_part, "ep", axis=1, tiled=True)
    matches = routes[:, :, None] == jnp.arange(devices, dtype=jnp.int32)[None, None, :]
    member = jnp.sum(matches.astype(jnp.int32), axis=1)
    weight_of = jnp.sum(jnp.where(matches, route_weight[:, :, None], 0.0), axis=1)
    slot_rank = jnp.cumsum(member, axis=0) - member
    slot_ids = jnp.arange(CAP, dtype=jnp.int32)
    mine_member = lax.dynamic_slice_in_dim(member, device_rank, 1, 1)[:, 0]
    mine_slot = lax.dynamic_slice_in_dim(slot_rank, device_rank, 1, 1)[:, 0]
    chosen = (mine_slot[None, :] == slot_ids[:, None]) & (mine_member[None, :] == 1)
    taken_rows = jnp.dot(
        chosen.astype(jnp.bfloat16), first_rows, preferred_element_type=jnp.float32
    ).astype(jnp.bfloat16)
    expert_out = swiglu(taken_rows, expert_gate[0], expert_up[0], expert_down[0])
    arrived = lax.all_to_all(expert_out, "ep", split_axis=1, concat_axis=0, tiled=True)
    spread = jnp.where(
        (slot_rank[:, :, None] == slot_ids[None, None, :]) & (member[:, :, None] == 1),
        weight_of[:, :, None],
        0.0,
    )
    moe_part = jnp.dot(
        spread.reshape(row_count, devices * CAP),
        arrived.astype(jnp.float32),
        precision=lax.Precision.HIGHEST,
    )
    down_part = lax.dynamic_slice_in_dim(shared_down, column_start, slice_width, 1)
    shared_part = swiglu(first_rows, shared_gate, shared_up, down_part)
    moe_part = moe_part + shared_part.astype(jnp.float32)
    residual_two = RESIDUAL_SCALE * first_part.astype(jnp.float32) + moe_part
    total_two, square_two = lax.psum(
        (jnp.sum(residual_two, axis=1), jnp.sum(residual_two * residual_two, axis=1)), "ep"
    )
    result = finish_norm(residual_two, total_two, square_two, full_width, second_gain).astype(
        jnp.bfloat16
    )
    return (result, window[:, 1:], new_state.reshape(own_rows, head_count, HEAD_DIM, STATE))


def solution(mesh):
    return jax.shard_map(
        on_device,
        mesh=mesh,
        in_specs=(
            P("grp", "ep"),
            P(("grp", "ep"), None, None),
            P(("grp", "ep"), None, None, None),
            P("ep", None),
            P("ep", None),
            P("ep", None),
            P("ep", None),
            P("ep", None),
            P(),
            P(),
            P(),
            P(),
            P(),
            P(None, "ep"),
            P(),
            P("grp", None),
            P("grp", None),
            P("ep", None, None),
            P("ep", None, None),
            P("ep", None, None),
            P(),
            P(),
            P(),
            P("ep"),
        ),
        out_specs=(
            P("grp", "ep"),
            P(("grp", "ep"), None, None),
            P(("grp", "ep"), None, None, None),
        ),
        check_vma=False,
    )
```

profile of v0, /device:TPU:0, one launch (start us, length us, event | category | flops | bytes accessed | tf_op | source)
XLA Modules:
  0.0 191.0 jit_solution(8677031213126030681)
XLA Ops:
  0.7 0.7 copy-done.7
  1.4 1.3 convolution_dynamic-update-slice_fusion.1
  2.7 0.2 convolution_dynamic-update-slice_fusion
  2.9 1.0 convolution_dynamic-update-slice_fusion.3
  3.9 1.0 convolution_dynamic-update-slice_fusion.2
  4.9 0.8 convolution_dynamic-update-slice_fusion.4
  5.7 66.2 %all-reduce.4 = bf16[16,4640]{1,0:T(8,128)(2,1)S(1)} all-reduce(f32[16,4640]{1,0:T(8,128)S(1)} %convolution_dynamic-update-slice_fusion.4), channel_id=3, replica_groups=mesh['grp'=2,'ep'=16] {'ep'}, use_global_device_ids=true, to_apply=%region_0.0.clone | all-reduce | flops 74240 | bytes 445440
  71.9 0.6 copy-done.17
  72.6 0.6 dynamic-slice
  73.1 0.7 dynamic-slice_convert_fusion
  73.9 0.7 copy-done.8
  74.8 0.6 copy-done.14
  75.5 1.4 multiply_reduce_fusion
  77.4 0.5 broadcast.167
  77.9 0.7 fusion.47
  78.8 17.3 %all-gather = bf16[32768]{0:T(1024)(128)(2,1)S(1)} all-gather(bf16[2048]{0:T(1024)(128)(2,1)S(1)} %multiply_convert_fusion.2), channel_id=2, replica_groups=mesh['grp'=2,'ep'=16] {'ep'}, dimensions={0}, use_global_device_ids=true | all-gather | bytes 69632 | tf_op jit(solution)/shard_map/all_gather | solution.py:119
  96.2 1.3 convolution_convert_fusion.2
  97.6 0.8 dynamic_slice.12
  98.4 31.4 %all-reduce.2 = (f32[16]{0:T(128)S(1)}, f32[16]{0:T(128)S(1)}) all-reduce(f32[16]{0:T(128)S(1)} %get-tuple-element.6, f32[16]{0:T(128)S(1)} %get-tuple-element.5), channel_id=1, replica_groups=mesh['grp'=2,'ep'=16] {'ep'}, use_global_device_ids=true, to_apply=%region_7.8 | all-reduce | flops 32 | bytes 256 | tf_op jit(solution)/shard_map/psum | solution.py:126
  129.9 17.3 %all_gather.7 = bf16[16,2048]{1,0:T(8,128)(2,1)S(1)} all-gather(bf16[16,128]{1,0:T(8,128)(2,1)S(1)} %multiply_convert_fusion.1), channel_id=1, replica_groups=mesh['grp'=2,'ep'=16] {'ep'}, dimensions={1}, use_global_device_ids=true | all-gather | bytes 69632 | tf_op jit(solution)/shard_map/all_gather | solution.py:131
  147.3 0.2 fusion.32
  147.8 0.2 fusion.9
  148.1 1.3 convolution_convert_fusion
  149.4 3.6 %all-to-all-start = ((bf16[8,16,128]{2,0,1:T(8,128)(2,1)}), bf16[8,16,128]{2,0,1:T(8,128)(2,1)S(1)}, u32[]{:S(2)}, u32[]{:S(2)}) async-start(bf16[8,16,128]{2,0,1:T(8,128)(2,1)} %bitcast.13), calls=%async_computation | async-start | bytes 65536 | tf_op jit(solution)/shard_map/all_to_all | solution.py:144
  153.0 0.2 fusion.50
  153.3 1.2 fusion.5
  154.5 0.7 pad_maximum_fusion
  155.3 4.3 %all-to-all-done = bf16[8,16,128]{2,0,1:T(8,128)(2,1)S(1)} async-done(((bf16[8,16,128]{2,0,1:T(8,128)(2,1)}), bf16[8,16,128]{2,0,1:T(8,128)(2,1)S(1)}, u32[]{:S(2)}, u32[]{:S(2)}) %all-to-all-start) | async-done | bytes 32800 | tf_op jit(solution)/shard_map/all_to_all | solution.py:144
  159.6 0.4 fusion.45
  160.0 29.7 %all-reduce.1 = (f32[16]{0:T(128)S(1)}, f32[16]{0:T(128)S(1)}) all-reduce(f32[16]{0:T(128)S(1)} %get-tuple-element.4, f32[16]{0:T(128)S(1)} %get-tuple-element.3), channel_id=1, replica_groups=mesh['grp'=2,'ep'=16] {'ep'}, use_global_device_ids=true, to_apply=%region_14.15 | all-reduce | flops 32 | bytes 256 | tf_op jit(solution)/shard_map/psum | solution.py:159
  189.7 0.7 copy-done.13
  190.3 0.7 multiply_convert_fusion
  (65 shorter events, 1.9 us)
Async XLA Ops:
  0.6 147.4 %copy-start = (bf16[1,256,2048]{2,1,0:T(8,128)(2,1)S(1)}, bf16[1,256,2048]{2,1,0:T(8,128)(2,1)}, u32[]{:S(2)}) copy-start(bf16[1,256,2048]{2,1,0:T(8,128)(2,1)} %param.43) | copy-start | bytes 3145732
  0.6 0.8 copy-start.7
  0.7 2.1 %copy-start.6 = (bf16[128,2048]{1,0:T(8,128)(2,1)S(1)}, bf16[128,2048]{1,0:T(8,128)(2,1)}, u32[]{:S(2)}) copy-start(bf16[128,2048]{1,0:T(8,128)(2,1)} %param.28) | copy-start | bytes 1572868
  1.4 74.1 %copy-start.1 = (f32[1,32,64,128]{3,2,1,0:T(8,128)S(1)}, f32[1,32,64,128]{3,2,1,0:T(8,128)}, u32[]{:S(2)}) copy-start(f32[1,32,64,128]{3,2,1,0:T(8,128)} %param.26) | copy-start | bytes 3145732
  71.9 0.7 copy-start.17
  73.1 0.7 copy-start.9
  73.8 0.7 copy-start.8
  74.7 0.7 copy-start.14
  74.7 0.7 copy-start.15
  75.5 1.6 copy-start.16
  75.5 3.3 %copy-start.11 = (f32[2048]{0:T(1024)S(1)}, f32[2048]{0:T(1024)}, u32[]{:S(2)}) copy-start(f32[2048]{0:T(1024)} %param.36) | copy-start | bytes 24580
  76.9 70.9 %copy-start.2 = (bf16[1,2048,256]{2,1,0:T(8,128)(2,1)S(1)}, bf16[1,2048,256]{2,1,0:T(8,128)(2,1)}, u32[]{:S(2)}) copy-start(bf16[1,2048,256]{2,1,0:T(8,128)(2,1)} %param.41) | copy-start | bytes 3145732
  78.8 68.3 %copy-start.10 = (s32[16,4]{0,1:T(4,128)S(1)}, s32[16,4]{0,1:T(4,128)}, u32[]{:S(2)}) copy-start(s32[16,4]{0,1:T(4,128)} %param.39) | copy-start | bytes 772
  96.1 51.9 %copy-start.3 = (bf16[1,2048,256]{2,1,0:T(8,128)(2,1)S(1)}, bf16[1,2048,256]{2,1,0:T(8,128)(2,1)}, u32[]{:S(2)}) copy-start(bf16[1,2048,256]{2,1,0:T(8,128)(2,1)} %param.42) | copy-start | bytes 3145732
  148.0 5.0 %copy-start.4 = (bf16[2048,256]{1,0:T(8,128)(2,1)S(1)}, bf16[2048,256]{1,0:T(8,128)(2,1)}, u32[]{:S(2)}) copy-start(bf16[2048,256]{1,0:T(8,128)(2,1)} %param.44) | copy-start | bytes 3145732
  149.4 3.9 %copy-start.5 = (bf16[2048,256]{1,0:T(8,128)(2,1)S(1)}, bf16[2048,256]{1,0:T(8,128)(2,1)}, u32[]{:S(2)}) copy-start(bf16[2048,256]{1,0:T(8,128)(2,1)} %param.45) | copy-start | bytes 3145732
  149.4 10.2 %all-to-all-start = ((bf16[8,16,128]{2,0,1:T(8,128)(2,1)}), bf16[8,16,128]{2,0,1:T(8,128)(2,1)S(1)}, u32[]{:S(2)}, u32[]{:S(2)}) async-start(bf16[8,16,128]{2,0,1:T(8,128)(2,1)} %bitcast.13), calls=%async_computation | async-start | bytes 65536 | tf_op jit(solution)/shard_map/all_to_all | solution.py:144
  154.5 0.7 copy-start.12
  189.7 0.7 copy-start.13
where the time goes:
time: 192 us; the launch traced here: 191 us
  blocking collectives  162 us (84%)
  matrix products  9.08 us (5%)
  local copies, waits for them, and re-layouts  6.89 us (4%)
  waiting for transfers between devices  4.33 us (2%)
  other arithmetic  4.32 us (2%)
  starting transfers between devices  3.63 us (2%)
    unnamed x1, blocking collectives  66.2 us
    psum x1, blocking collectives, on_device(): lax.psum((jnp.sum(residual, axis=1), jnp.sum(residual * residual, axis=1)...  31.4 us
    psum x1, blocking collectives, on_device(): lax.psum((jnp.sum(residual_two, axis=1), jnp.sum(residual_two * residual_...  29.7 us
    all_gather x1, blocking collectives, on_device(): lax.all_gather(normed, 'ep', axis=0, tiled=True)  17.3 us
    all_gather x1, blocking collectives, on_device(): first_rows = lax.all_gather(first_part, 'ep', axis=1, tiled=True)  17.3 us
    all_to_all x1, waiting for transfers between devices, on_device(): lax.all_to_all(expert_out, 'ep', split_axis=1, concat_axis=0, tiled=True)  4.33 us
    dot_general x5, matrix products, on_device(): jnp.dot(stream, weight, preferred_element_type=jnp.float32)  4.26 us
    unnamed x37, local copies, waits for them, and re-layouts  4.03 us
  transfers between devices with their start and end apart: 1, of which 1 were waited for; matrix products, arithmetic and copies ran while one was open for 1% of the time, Pallas kernels for 0%

commit v1 on v0

--- a/solution.py
+++ b/solution.py
@@ -10,6 +10,19 @@
 RESIDUAL_SCALE = 2.0**0.25
 NORM_EPSILON = 1e-05
 GATED_EPSILON = 1e-06
+
+
+def ring_gather(x, axis, dim):
+    ways = lax.axis_size(axis)
+    up = [(d, (d + 1) % ways) for d in range(ways)]
+    down = [(d, (d - 1) % ways) for d in range(ways)]
+    earlier, later = ([x], [x])
+    for _ in range(ways // 2):
+        earlier.append(lax.ppermute(earlier[-1], axis, up))
+    for _ in range((ways - 1) // 2):
+        later.append(lax.ppermute(later[-1], axis, down))
+    line = jnp.concatenate([*earlier[::-1], *later[1:]], axis=dim)
+    return jnp.roll(line, (lax.axis_index(axis) - ways // 2) * x.shape[dim], axis=dim)
 
 
 def rounded(value):
@@ -115,11 +128,7 @@
     )
     normed = (normed.reshape(own_rows, inner_width) * group_gain).astype(jnp.bfloat16)
     mixer_out = rounded(
-        jnp.dot(
-            lax.all_gather(normed, "ep", axis=0, tiled=True),
-            out_weight,
-            preferred_element_type=jnp.float32,
-        )
+        jnp.dot(ring_gather(normed, "ep", 0), out_weight, preferred_element_type=jnp.float32)
     )
     column_start = device_rank * slice_width
     residual = RESIDUAL_SCALE * stream.astype(jnp.float32) + mixer_out.astype(jnp.float32)

time: 192 us -> 218 us (1.14)
  starting transfers between devices: 3.63 us -> 34.6 us
  blocking collectives: 162 us -> 143 us
  waiting for transfers between devices: 4.33 us -> 18.3 us
    ppermute x0 -> x15, starting transfers between devices: none -> 31 us  [the longest x7 30.9 us: ring_gather(): later.append(lax.ppermute(later[-1], axis, down))]
    all_gather x1 -> x0, blocking collectives: 17.3 us -> none  [on_device(): lax.all_gather(normed, 'ep', axis=0, tiled=True)]
    ppermute x0 -> x15, waiting for transfers between devices: none -> 13.2 us  [the longest x8 11.8 us: ring_gather(): earlier.append(lax.ppermute(earlier[-1], axis, up))]
  transfers between devices with their start and end apart: 1 -> 16, of which waited for: 1 -> 11; matrix products, arithmetic and copies ran while one was open for 1% -> 2% of each run, Pallas kernels for 0% -> 0%
where the time goes in v1:
time: 218 us; the launch traced here: 217 us
  blocking collectives  143 us (66%)
  starting transfers between devices  34.6 us (16%)
  waiting for transfers between devices  18.3 us (8%)
  matrix products  9 us (4%)
  local copies, waits for them, and re-layouts  7.26 us (3%)
  other arithmetic  4.3 us (2%)
    unnamed x1, blocking collectives  66.2 us
    ppermute x7, starting transfers between devices, ring_gather(): later.append(lax.ppermute(later[-1], axis, down))  30.9 us
    psum x1, blocking collectives, on_device(): lax.psum((jnp.sum(residual_two, axis=1), jnp.sum(residual_two * residual_...  29.7 us
    psum x1, blocking collectives, on_device(): lax.psum((jnp.sum(residual, axis=1), jnp.sum(residual * residual, axis=1)...  29.5 us
    all_gather x1, blocking collectives, on_device(): first_rows = lax.all_gather(first_part, 'ep', axis=1, tiled=True)  17.3 us
    ppermute x8, waiting for transfers between devices, ring_gather(): earlier.append(lax.ppermute(earlier[-1], axis, up))  11.8 us
    all_to_all x1, waiting for transfers between devices, on_device(): lax.all_to_all(expert_out, 'ep', split_axis=1, concat_axis=0, tiled=True)  5.13 us
  transfers between devices with their start and end apart: 16, of which 11 were waited for; matrix products, arithmetic and copies ran while one was open for 2% of the time, Pallas kernels for 0%

profile of v1, /device:TPU:0, one launch (start us, length us, event | category | flops | bytes accessed | tf_op | source)
XLA Modules:
  0.0 217.1 jit_solution(16144294664697852760)
XLA Ops:
  0.7 0.7 copy-done.7
  1.4 1.3 convolution_dynamic-update-slice_fusion.1
  2.9 1.0 convolution_dynamic-update-slice_fusion.3
  3.9 1.0 convolution_dynamic-update-slice_fusion.2
  4.9 0.8 convolution_dynamic-update-slice_fusion.4
  5.7 66.2 %all-reduce.4 = bf16[16,4640]{1,0:T(8,128)(2,1)S(1)} all-reduce(f32[16,4640]{1,0:T(8,128)S(1)} %convolution_dynamic-update-slice_fusion.4), channel_id=2, replica_groups=mesh['grp'=2,'ep'=16] {'ep'}, use_global_device_ids=true, to_apply=%region_0.0.clone | all-reduce | flops 74240 | bytes 445440
  75.5 1.4 multiply_reduce_fusion
  77.9 0.7 fusion.49
  78.9 4.4 %collective-permute-start.8 = (bf16[1,2048]{1,0:T(2,128)(2,1)S(1)}, bf16[1,2048]{1,0:T(2,128)(2,1)S(1)}, u32[]{:S(2)}, u32[]{:S(2)}) collective-permute-start(bf16[1,2048]{1,0:T(2,128)(2,1)S(1)} %convert_element_type.70), channel_id=1, source_target_pairs={{0,15},{1,0},{2,1},{3,2},{4,3},{5,4},{6,5},{7,6},{8,7},{9,8},{10,9... | collective-permute-start | bytes 12296 | tf_op jit(solution)/shard_map/ppermute | solution.py:23
  83.4 1.3 collective-permute-done
  84.7 4.4 %collective-permute-start.9 = (bf16[1,2048]{1,0:T(2,128)(2,1)S(1)}, bf16[1,2048]{1,0:T(2,128)(2,1)S(1)}, u32[]{:S(2)}, u32[]{:S(2)}) collective-permute-start(bf16[1,2048]{1,0:T(2,128)(2,1)S(1)} %collective-permute-done.8), channel_id=1, source_target_pairs={{0,15},{1,0},{2,1},{3,2},{4,3},{5,4},{6,5},{7,6},{8,7},{9,8},{10,9... | collective-permute-start | bytes 12296 | tf_op jit(solution)/shard_map/ppermute | solution.py:23
  89.1 1.3 collective-permute-done.1
  90.5 4.4 %collective-permute-start.10 = (bf16[1,2048]{1,0:T(2,128)(2,1)S(1)}, bf16[1,2048]{1,0:T(2,128)(2,1)S(1)}, u32[]{:S(2)}, u32[]{:S(2)}) collective-permute-start(bf16[1,2048]{1,0:T(2,128)(2,1)S(1)} %collective-permute-done.9), channel_id=1, source_target_pairs={{0,15},{1,0},{2,1},{3,2},{4,3},{5,4},{6,5},{7,6},{8,7},{9,8},{10,9... | collective-permute-start | bytes 12296 | tf_op jit(solution)/shard_map/ppermute | solution.py:23
  94.9 1.3 collective-permute-done.2
  96.3 4.4 %collective-permute-start.11 = (bf16[1,2048]{1,0:T(2,128)(2,1)S(1)}, bf16[1,2048]{1,0:T(2,128)(2,1)S(1)}, u32[]{:S(2)}, u32[]{:S(2)}) collective-permute-start(bf16[1,2048]{1,0:T(2,128)(2,1)S(1)} %collective-permute-done.10), channel_id=1, source_target_pairs={{0,15},{1,0},{2,1},{3,2},{4,3},{5,4},{6,5},{7,6},{8,7},{9,8},{10,9... | collective-permute-start | bytes 12296 | tf_op jit(solution)/shard_map/ppermute | solution.py:23
  100.7 1.3 collective-permute-done.3
  102.7 4.4 %collective-permute-start.12 = (bf16[1,2048]{1,0:T(2,128)(2,1)S(1)}, bf16[1,2048]{1,0:T(2,128)(2,1)S(1)}, u32[]{:S(2)}, u32[]{:S(2)}) collective-permute-start(bf16[1,2048]{1,0:T(2,128)(2,1)S(1)} %collective-permute-done.11), channel_id=1, source_target_pairs={{0,15},{1,0},{2,1},{3,2},{4,3},{5,4},{6,5},{7,6},{8,7},{9,8},{10,9... | collective-permute-start | bytes 12296 | tf_op jit(solution)/shard_map/ppermute | solution.py:23
  107.1 0.7 collective-permute-done.4
  108.5 4.4 %collective-permute-start.13 = (bf16[1,2048]{1,0:T(2,128)(2,1)S(1)}, bf16[1,2048]{1,0:T(2,128)(2,1)S(1)}, u32[]{:S(2)}, u32[]{:S(2)}) collective-permute-start(bf16[1,2048]{1,0:T(2,128)(2,1)S(1)} %collective-permute-done.12), channel_id=1, source_target_pairs={{0,15},{1,0},{2,1},{3,2},{4,3},{5,4},{6,5},{7,6},{8,7},{9,8},{10,9... | collective-permute-start | bytes 12296 | tf_op jit(solution)/shard_map/ppermute | solution.py:23
  112.9 0.7 collective-permute-done.5
  114.2 4.4 %collective-permute-start.14 = (bf16[1,2048]{1,0:T(2,128)(2,1)S(1)}, bf16[1,2048]{1,0:T(2,128)(2,1)S(1)}, u32[]{:S(2)}, u32[]{:S(2)}) collective-permute-start(bf16[1,2048]{1,0:T(2,128)(2,1)S(1)} %collective-permute-done.13), channel_id=1, source_target_pairs={{0,15},{1,0},{2,1},{3,2},{4,3},{5,4},{6,5},{7,6},{8,7},{9,8},{10,9... | collective-permute-start | bytes 12296 | tf_op jit(solution)/shard_map/ppermute | solution.py:23
  118.6 0.7 collective-permute-done.6
  119.5 0.8 dynamic_slice.17
  120.7 4.4 %collective-permute-done.7 = bf16[1,2048]{1,0:T(2,128)(2,1)S(1)} collective-permute-done((bf16[1,2048]{1,0:T(2,128)(2,1)S(1)}, bf16[1,2048]{1,0:T(2,128)(2,1)S(1)}, u32[]{:S(2)}, u32[]{:S(2)}) %collective-permute-start.7) | collective-permute-done | bytes 4128 | tf_op jit(solution)/shard_map/ppermute | solution.py:21
  125.5 1.2 convolution_convert_fusion.2
  126.9 29.5 %all-reduce.2 = (f32[16]{0:T(128)S(1)}, f32[16]{0:T(128)S(1)}) all-reduce(f32[16]{0:T(128)S(1)} %get-tuple-element.6, f32[16]{0:T(128)S(1)} %get-tuple-element.5), channel_id=1, replica_groups=mesh['grp'=2,'ep'=16] {'ep'}, use_global_device_ids=true, to_apply=%region_7.8 | all-reduce | flops 32 | bytes 256 | tf_op jit(solution)/shard_map/psum | solution.py:135
  156.5 17.3 %all_gather.3 = bf16[16,2048]{1,0:T(8,128)(2,1)S(1)} all-gather(bf16[16,128]{1,0:T(8,128)(2,1)S(1)} %multiply_convert_fusion.1), channel_id=1, replica_groups=mesh['grp'=2,'ep'=16] {'ep'}, dimensions={1}, use_global_device_ids=true | all-gather | bytes 69632 | tf_op jit(solution)/shard_map/all_gather | solution.py:140
  174.2 1.3 convolution_convert_fusion
  175.5 3.6 %all-to-all-start = ((bf16[8,16,128]{2,0,1:T(8,128)(2,1)}), bf16[8,16,128]{2,0,1:T(8,128)(2,1)S(1)}, u32[]{:S(2)}, u32[]{:S(2)}) async-start(bf16[8,16,128]{2,0,1:T(8,128)(2,1)} %bitcast.13), calls=%async_computation | async-start | bytes 65536 | tf_op jit(solution)/shard_map/all_to_all | solution.py:153
  179.4 1.2 fusion.5
  180.6 5.1 %all-to-all-done = bf16[8,16,128]{2,0,1:T(8,128)(2,1)S(1)} async-done(((bf16[8,16,128]{2,0,1:T(8,128)(2,1)}), bf16[8,16,128]{2,0,1:T(8,128)(2,1)S(1)}, u32[]{:S(2)}, u32[]{:S(2)}) %all-to-all-start) | async-done | bytes 32800 | tf_op jit(solution)/shard_map/all_to_all | solution.py:153
  186.1 29.7 %all-reduce.1 = (f32[16]{0:T(128)S(1)}, f32[16]{0:T(128)S(1)}) all-reduce(f32[16]{0:T(128)S(1)} %get-tuple-element.4, f32[16]{0:T(128)S(1)} %get-tuple-element.3), channel_id=1, replica_groups=mesh['grp'=2,'ep'=16] {'ep'}, use_global_device_ids=true, to_apply=%region_14.15 | all-reduce | flops 32 | bytes 256 | tf_op jit(solution)/shard_map/psum | solution.py:168
  (95 shorter events, 10.6 us)
Async XLA Ops:
  0.6 173.5 %copy-start = (bf16[1,256,2048]{2,1,0:T(8,128)(2,1)S(1)}, bf16[1,256,2048]{2,1,0:T(8,128)(2,1)}, u32[]{:S(2)}) copy-start(bf16[1,256,2048]{2,1,0:T(8,128)(2,1)} %param.43) | copy-start | bytes 3145732
  0.6 0.8 copy-start.7
  0.7 2.1 copy-start.6
  1.4 74.1 %copy-start.1 = (f32[1,32,64,128]{3,2,1,0:T(8,128)S(1)}, f32[1,32,64,128]{3,2,1,0:T(8,128)}, u32[]{:S(2)}) copy-start(f32[1,32,64,128]{3,2,1,0:T(8,128)} %param.26) | copy-start | bytes 3145732
  73.1 0.7 copy-start.9
  73.8 0.7 copy-start.8
  74.7 0.7 copy-start.15
  75.5 1.6 copy-start.16
  75.5 3.3 %copy-start.11 = (f32[2048]{0:T(1024)S(1)}, f32[2048]{0:T(1024)}, u32[]{:S(2)}) copy-start(f32[2048]{0:T(1024)} %param.36) | copy-start | bytes 24580
  75.5 32.3 %copy-start.10 = (s32[16,4]{0,1:T(4,128)S(1)}, s32[16,4]{0,1:T(4,128)}, u32[]{:S(2)}) copy-start(s32[16,4]{0,1:T(4,128)} %param.39) | copy-start | bytes 772
  75.5 43.8 %copy-start.12 = (f32[16,4]{0,1:T(4,128)S(1)}, f32[16,4]{0,1:T(4,128)}, u32[]{:S(2)}) copy-start(f32[16,4]{0,1:T(4,128)} %param.40) | copy-start | bytes 772
  76.9 97.0 %copy-start.2 = (bf16[1,2048,256]{2,1,0:T(8,128)(2,1)S(1)}, bf16[1,2048,256]{2,1,0:T(8,128)(2,1)}, u32[]{:S(2)}) copy-start(bf16[1,2048,256]{2,1,0:T(8,128)(2,1)} %param.41) | copy-start | bytes 3145732
  78.9 5.8 %collective-permute-start = (bf16[1,2048]{1,0:T(2,128)(2,1)S(1)}, bf16[1,2048]{1,0:T(2,128)(2,1)S(1)}, u32[]{:S(2)}, u32[]{:S(2)}) collective-permute-start(bf16[1,2048]{1,0:T(2,128)(2,1)S(1)} %convert_element_type.70), channel_id=1, source_target_pairs={{0,1},{1,2},{2,3},{3,4},{4,5},{5,6},{6,7},{7,8},{8,9},{9,10},{10,1... | collective-permute-start | bytes 12296 | tf_op jit(solution)/shard_map/ppermute | solution.py:21
  78.9 5.8 %collective-permute-start.8 = (bf16[1,2048]{1,0:T(2,128)(2,1)S(1)}, bf16[1,2048]{1,0:T(2,128)(2,1)S(1)}, u32[]{:S(2)}, u32[]{:S(2)}) collective-permute-start(bf16[1,2048]{1,0:T(2,128)(2,1)S(1)} %convert_element_type.70), channel_id=1, source_target_pairs={{0,15},{1,0},{2,1},{3,2},{4,3},{5,4},{6,5},{7,6},{8,7},{9,8},{10,9... | collective-permute-start | bytes 12296 | tf_op jit(solution)/shard_map/ppermute | solution.py:23
  84.7 5.8 %collective-permute-start.1 = (bf16[1,2048]{1,0:T(2,128)(2,1)S(1)}, bf16[1,2048]{1,0:T(2,128)(2,1)S(1)}, u32[]{:S(2)}, u32[]{:S(2)}) collective-permute-start(bf16[1,2048]{1,0:T(2,128)(2,1)S(1)} %collective-permute-done), channel_id=1, source_target_pairs={{0,1},{1,2},{2,3},{3,4},{4,5},{5,6},{6,7},{7,8},{8,9},{9,10},{10,1... | collective-permute-start | bytes 12296 | tf_op jit(solution)/shard_map/ppermute | solution.py:21
  84.7 5.8 %collective-permute-start.9 = (bf16[1,2048]{1,0:T(2,128)(2,1)S(1)}, bf16[1,2048]{1,0:T(2,128)(2,1)S(1)}, u32[]{:S(2)}, u32[]{:S(2)}) collective-permute-start(bf16[1,2048]{1,0:T(2,128)(2,1)S(1)} %collective-permute-done.8), channel_id=1, source_target_pairs={{0,15},{1,0},{2,1},{3,2},{4,3},{5,4},{6,5},{7,6},{8,7},{9,8},{10,9... | collective-permute-start | bytes 12296 | tf_op jit(solution)/shard_map/ppermute | solution.py:23
  90.5 5.8 %collective-permute-start.2 = (bf16[1,2048]{1,0:T(2,128)(2,1)S(1)}, bf16[1,2048]{1,0:T(2,128)(2,1)S(1)}, u32[]{:S(2)}, u32[]{:S(2)}) collective-permute-start(bf16[1,2048]{1,0:T(2,128)(2,1)S(1)} %collective-permute-done.1), channel_id=1, source_target_pairs={{0,1},{1,2},{2,3},{3,4},{4,5},{5,6},{6,7},{7,8},{8,9},{9,10},{10,1... | collective-permute-start | bytes 12296 | tf_op jit(solution)/shard_map/ppermute | solution.py:21
  90.5 5.8 %collective-permute-start.10 = (bf16[1,2048]{1,0:T(2,128)(2,1)S(1)}, bf16[1,2048]{1,0:T(2,128)(2,1)S(1)}, u32[]{:S(2)}, u32[]{:S(2)}) collective-permute-start(bf16[1,2048]{1,0:T(2,128)(2,1)S(1)} %collective-permute-done.9), channel_id=1, source_target_pairs={{0,15},{1,0},{2,1},{3,2},{4,3},{5,4},{6,5},{7,6},{8,7},{9,8},{10,9... | collective-permute-start | bytes 12296 | tf_op jit(solution)/shard_map/ppermute | solution.py:23
  96.2 5.8 %collective-permute-start.3 = (bf16[1,2048]{1,0:T(2,128)(2,1)S(1)}, bf16[1,2048]{1,0:T(2,128)(2,1)S(1)}, u32[]{:S(2)}, u32[]{:S(2)}) collective-permute-start(bf16[1,2048]{1,0:T(2,128)(2,1)S(1)} %collective-permute-done.2), channel_id=1, source_target_pairs={{0,1},{1,2},{2,3},{3,4},{4,5},{5,6},{6,7},{7,8},{8,9},{9,10},{10,1... | collective-permute-start | bytes 12296 | tf_op jit(solution)/shard_map/ppermute | solution.py:21
  96.3 6.4 %collective-permute-start.11 = (bf16[1,2048]{1,0:T(2,128)(2,1)S(1)}, bf16[1,2048]{1,0:T(2,128)(2,1)S(1)}, u32[]{:S(2)}, u32[]{:S(2)}) collective-permute-start(bf16[1,2048]{1,0:T(2,128)(2,1)S(1)} %collective-permute-done.10), channel_id=1, source_target_pairs={{0,15},{1,0},{2,1},{3,2},{4,3},{5,4},{6,5},{7,6},{8,7},{9,8},{10,9... | collective-permute-start | bytes 12296 | tf_op jit(solution)/shard_map/ppermute | solution.py:23
  102.0 5.8 %collective-permute-start.4 = (bf16[1,2048]{1,0:T(2,128)(2,1)S(1)}, bf16[1,2048]{1,0:T(2,128)(2,1)S(1)}, u32[]{:S(2)}, u32[]{:S(2)}) collective-permute-start(bf16[1,2048]{1,0:T(2,128)(2,1)S(1)} %collective-permute-done.3), channel_id=1, source_target_pairs={{0,1},{1,2},{2,3},{3,4},{4,5},{5,6},{6,7},{7,8},{8,9},{9,10},{10,1... | collective-permute-start | bytes 12296 | tf_op jit(solution)/shard_map/ppermute | solution.py:21
  102.7 5.8 %collective-permute-start.12 = (bf16[1,2048]{1,0:T(2,128)(2,1)S(1)}, bf16[1,2048]{1,0:T(2,128)(2,1)S(1)}, u32[]{:S(2)}, u32[]{:S(2)}) collective-permute-start(bf16[1,2048]{1,0:T(2,128)(2,1)S(1)} %collective-permute-done.11), channel_id=1, source_target_pairs={{0,15},{1,0},{2,1},{3,2},{4,3},{5,4},{6,5},{7,6},{8,7},{9,8},{10,9... | collective-permute-start | bytes 12296 | tf_op jit(solution)/shard_map/ppermute | solution.py:23
  107.8 5.8 %collective-permute-start.5 = (bf16[1,2048]{1,0:T(2,128)(2,1)S(1)}, bf16[1,2048]{1,0:T(2,128)(2,1)S(1)}, u32[]{:S(2)}, u32[]{:S(2)}) collective-permute-start(bf16[1,2048]{1,0:T(2,128)(2,1)S(1)} %collective-permute-done.4), channel_id=1, source_target_pairs={{0,1},{1,2},{2,3},{3,4},{4,5},{5,6},{6,7},{7,8},{8,9},{9,10},{10,1... | collective-permute-start | bytes 12296 | tf_op jit(solution)/shard_map/ppermute | solution.py:21
  108.5 5.8 %collective-permute-start.13 = (bf16[1,2048]{1,0:T(2,128)(2,1)S(1)}, bf16[1,2048]{1,0:T(2,128)(2,1)S(1)}, u32[]{:S(2)}, u32[]{:S(2)}) collective-permute-start(bf16[1,2048]{1,0:T(2,128)(2,1)S(1)} %collective-permute-done.12), channel_id=1, source_target_pairs={{0,15},{1,0},{2,1},{3,2},{4,3},{5,4},{6,5},{7,6},{8,7},{9,8},{10,9... | collective-permute-start | bytes 12296 | tf_op jit(solution)/shard_map/ppermute | solution.py:23
  113.6 5.8 %collective-permute-start.6 = (bf16[1,2048]{1,0:T(2,128)(2,1)S(1)}, bf16[1,2048]{1,0:T(2,128)(2,1)S(1)}, u32[]{:S(2)}, u32[]{:S(2)}) collective-permute-start(bf16[1,2048]{1,0:T(2,128)(2,1)S(1)} %collective-permute-done.5), channel_id=1, source_target_pairs={{0,1},{1,2},{2,3},{3,4},{4,5},{5,6},{6,7},{7,8},{8,9},{9,10},{10,1... | collective-permute-start | bytes 12296 | tf_op jit(solution)/shard_map/ppermute | solution.py:21
  114.2 6.4 %collective-permute-start.14 = (bf16[1,2048]{1,0:T(2,128)(2,1)S(1)}, bf16[1,2048]{1,0:T(2,128)(2,1)S(1)}, u32[]{:S(2)}, u32[]{:S(2)}) collective-permute-start(bf16[1,2048]{1,0:T(2,128)(2,1)S(1)} %collective-permute-done.13), channel_id=1, source_target_pairs={{0,15},{1,0},{2,1},{3,2},{4,3},{5,4},{6,5},{7,6},{8,7},{9,8},{10,9... | collective-permute-start | bytes 12296 | tf_op jit(solution)/shard_map/ppermute | solution.py:23
  119.3 5.8 %collective-permute-start.7 = (bf16[1,2048]{1,0:T(2,128)(2,1)S(1)}, bf16[1,2048]{1,0:T(2,128)(2,1)S(1)}, u32[]{:S(2)}, u32[]{:S(2)}) collective-permute-start(bf16[1,2048]{1,0:T(2,128)(2,1)S(1)} %collective-permute-done.6), channel_id=1, source_target_pairs={{0,1},{1,2},{2,3},{3,4},{4,5},{5,6},{6,7},{7,8},{8,9},{9,10},{10,1... | collective-permute-start | bytes 12296 | tf_op jit(solution)/shard_map/ppermute | solution.py:21
  120.6 53.5 %copy-start.3 = (bf16[1,2048,256]{2,1,0:T(8,128)(2,1)S(1)}, bf16[1,2048,256]{2,1,0:T(8,128)(2,1)}, u32[]{:S(2)}) copy-start(bf16[1,2048,256]{2,1,0:T(8,128)(2,1)} %param.42) | copy-start | bytes 3145732
  174.2 5.0 %copy-start.4 = (bf16[2048,256]{1,0:T(8,128)(2,1)S(1)}, bf16[2048,256]{1,0:T(8,128)(2,1)}, u32[]{:S(2)}) copy-start(bf16[2048,256]{1,0:T(8,128)(2,1)} %param.44) | copy-start | bytes 3145732
  175.5 3.9 %copy-start.5 = (bf16[2048,256]{1,0:T(8,128)(2,1)S(1)}, bf16[2048,256]{1,0:T(8,128)(2,1)}, u32[]{:S(2)}) copy-start(bf16[2048,256]{1,0:T(8,128)(2,1)} %param.45) | copy-start | bytes 3145732
  175.5 10.2 %all-to-all-start = ((bf16[8,16,128]{2,0,1:T(8,128)(2,1)}), bf16[8,16,128]{2,0,1:T(8,128)(2,1)S(1)}, u32[]{:S(2)}, u32[]{:S(2)}) async-start(bf16[8,16,128]{2,0,1:T(8,128)(2,1)} %bitcast.13), calls=%async_computation | async-start | bytes 65536 | tf_op jit(solution)/shard_map/all_to_all | solution.py:153
  215.8 0.7 copy-start.13
  (2 other events, 1.3 us)
